TPU v7x, 32 devices: a whole 2x2x4 slice. The times are simulated.
32 devices in a mesh: ep: 8 (over z, y), tp: 4 (over x, core).
Axes of the slice: x: 2, y: 2, z: 4, core: 2. Of those that a mesh axis runs over, the one named last changes fastest.
Arguments:
- query_rows: bfloat16 [2048, 2048], P('ep', 'tp'), may hold values from -6 to 6
- key_rows: bfloat16 [2048, 512], P('ep', 'tp'), may hold values from -18 to 18
- value_rows: bfloat16 [2048, 512], P('ep', 'tp'), may hold values from -12 to 12
- key_bias: bfloat16 [2048, 8], P('ep', 'tp'), may hold values from -2 to 13
- head_offset: float32 [32], P('tp'), may hold values from -16 to -3
- out_weight: bfloat16 [2048, 2048], P('tp'), may hold values from -0.125 to 0.125
- expert_input: bfloat16 [4096, 2048], P(('ep', 'tp')), may hold values from -40 to 40
- expert_gain: float32 [2048], replicated, may hold values from 0.1 to 1.9
- routes: int32 [4096, 2], P(('ep', 'tp')), may hold values from 0 to 7, all different within a row; in each aligned block of 128 rows (0 to 127, 128 to 255, ...) at most 48 rows name the same one
- route_weight: float32 [4096, 2], P(('ep', 'tp')), may hold values from 0.5 to 2
- gate_weight: bfloat16 [8, 2048, 3584], P('ep', None, 'tp'), may hold values from -0.125 to 0.125
- up_weight: bfloat16 [8, 2048, 3584], P('ep', None, 'tp'), may hold values from -0.125 to 0.125
- down_weight: bfloat16 [8, 3584, 2048], P('ep', 'tp'), may hold values from -0.09375 to 0.09375
Outputs:
- mixed_a: bfloat16 [2048, 2048], P(('ep', 'tp'))
- mixed_b: bfloat16 [4096, 2048], P(('ep', 'tp'))
Inputs may be any that keep to these rules, and one draw needn't show every extreme that they name: `routes`: each row names 2 different experts; in the rows of one device (aligned blocks of 128 rows) no expert is named more than 48 times, and in every draw some device names some expert exactly 48 times.
All inputs are finite; a program needn't handle non-finite values.
Results may differ from a plain program's by a relative error of at most 0.012.
Values may be sent and summed in bfloat16 or wider, within the bound.
A program may use at most 128 MiB of HBM per device.

v0:
```python
import math

import jax
import jax.numpy as jnp
from jax import lax
from jax.sharding import PartitionSpec as P

HD = 64


EPSILON = 1e-06


def rms_normed(rows, gain):
    values = rows.astype(jnp.float32)
    scaled = values * lax.rsqrt(jnp.mean(values * values, axis=-1, keepdims=True) + EPSILON)
    return (scaled * gain).astype(jnp.bfloat16)


def stick_update(running, queries4, key_tile_rows, value_block, bias_block, keep_mask, offsets):
    summed, survive = running
    kv_local = offsets.shape[0]
    key_heads = key_tile_rows.reshape(key_tile_rows.shape[0], kv_local, -1)
    value_heads = value_block.reshape(value_block.shape[0], kv_local, -1)
    head_dim = key_heads.shape[2]
    scores = jnp.einsum(
        "qgjd,kgd->gjqk", queries4, key_heads, preferred_element_type=jnp.float32
    ) * (1.0 / math.sqrt(head_dim))
    scores = (
        scores
        + offsets[:, :, None, None]
        + jnp.transpose(bias_block.astype(jnp.float32))[:, None, None, :]
    )
    log_stay = jnp.where(keep_mask, jax.nn.log_sigmoid(-scores), 0.0)
    after_sum = lax.cumsum(log_stay, axis=3, reverse=True) - log_stay + survive[..., None]
    weights = jnp.where(keep_mask, jnp.exp(jax.nn.log_sigmoid(scores) + after_sum), 0.0).astype(
        jnp.bfloat16
    )
    summed = summed + jnp.einsum(
        "gjqk,kgd->qgjd", weights, value_heads, preferred_element_type=jnp.float32
    )
    return (summed, survive + jnp.sum(log_stay, axis=3))


def body(
    query_rows,
    key_rows,
    value_rows,
    key_bias,
    head_offset,
    out_weight,
    expert_input,
    expert_gain,
    routes,
    route_weight,
    gate_weight,
    up_weight,
    down_weight,
):
    tok_rows = query_rows.shape[0]
    kv_local = key_rows.shape[1] // HD
    group_size = query_rows.shape[1] // key_rows.shape[1]
    offsets = head_offset.reshape(kv_local, group_size)
    all_keys, all_values, all_bias = (
        lax.all_gather(key_rows, "ep", axis=0, tiled=True),
        lax.all_gather(value_rows, "ep", axis=0, tiled=True),
        lax.all_gather(key_bias, "ep", axis=0, tiled=True),
    )
    key_span = min(512, all_keys.shape[0])
    position = lax.axis_index("ep") * tok_rows
    block_rows = query_rows.shape[0]
    queries4 = query_rows.reshape(block_rows, kv_local, group_size, HD)
    local_index = jnp.arange(block_rows)
    running = (
        jnp.zeros((block_rows, kv_local, group_size, HD), jnp.float32),
        jnp.zeros((kv_local, group_size, block_rows), jnp.float32),
    )
    own_keys = lax.dynamic_slice_in_dim(all_keys, position, block_rows, 0)
    own_values = lax.dynamic_slice_in_dim(all_values, position, block_rows, 0)
    own_bias = lax.dynamic_slice_in_dim(all_bias, position, block_rows, 0)
    running = stick_update(
        running,
        queries4,
        own_keys,
        own_values,
        own_bias,
        local_index[None, :] < local_index[:, None],
        offsets,
    )
    block_count = (position + key_span - 1) // key_span

    def remote_block(block_turn, state_pair):
        upper_row = position - block_turn * key_span
        first_row = jnp.maximum(upper_row - key_span, 0)
        key_tile_rows = lax.dynamic_slice_in_dim(all_keys, first_row, key_span, 0)
        value_block = lax.dynamic_slice_in_dim(all_values, first_row, key_span, 0)
        bias_block = lax.dynamic_slice_in_dim(all_bias, first_row, key_span, 0)
        keep_mask = jnp.broadcast_to(
            (first_row + jnp.arange(key_span) < upper_row)[None, :], (block_rows, key_span)
        )
        return stick_update(
            state_pair, queries4, key_tile_rows, value_block, bias_block, keep_mask, offsets
        )

    running = lax.fori_loop(0, block_count, remote_block, running)
    heads_out = running[0].reshape(block_rows, -1).astype(jnp.bfloat16)
    mixed_a = lax.psum_scatter(
        jnp.dot(heads_out, out_weight, preferred_element_type=jnp.float32).astype(jnp.bfloat16),
        "tp",
        scatter_dimension=0,
        tiled=True,
    )
    normed = rms_normed(expert_input, expert_gain)
    tok_count = normed.shape[0]
    top_count = routes.shape[1]
    model_width = normed.shape[1]
    expert_count = lax.axis_size("ep")
    capacity = max(2, 3 * tok_count * top_count // (2 * expert_count))
    flat_route = routes.reshape(-1)
    one_hot = (flat_route[:, None] == jnp.arange(expert_count)[None, :]).astype(jnp.int32)
    before = jnp.cumsum(one_hot, axis=0) - one_hot
    slot_index = (flat_route * capacity + jnp.sum(before * one_hot, axis=1)).reshape(
        tok_count, top_count
    )
    slot_ids = jnp.arange(expert_count * capacity)
    dispatch = jnp.sum(
        (slot_index[None, :, :] == slot_ids[:, None, None]).astype(jnp.int32), axis=2
    ).astype(jnp.bfloat16)
    outgoing = (
        jnp.dot(dispatch, normed, preferred_element_type=jnp.float32)
        .astype(jnp.bfloat16)
        .reshape(expert_count, capacity, model_width)
    )
    source_rows = expert_count * capacity
    arrived = lax.all_to_all(outgoing, "ep", split_axis=0, concat_axis=0, tiled=True)
    row_piece = lax.all_gather(arrived.reshape(source_rows, model_width), "tp", axis=0, tiled=True)
    gate_act = jnp.dot(row_piece, gate_weight[0], preferred_element_type=jnp.float32)
    up_act = jnp.dot(row_piece, up_weight[0], preferred_element_type=jnp.float32)
    hidden_all = (jax.nn.silu(gate_act) * up_act).astype(jnp.bfloat16)
    expert_result = lax.psum_scatter(
        jnp.dot(hidden_all, down_weight[0], preferred_element_type=jnp.float32).astype(
            jnp.bfloat16
        ),
        "tp",
        scatter_dimension=0,
        tiled=True,
    )
    returned = lax.all_to_all(
        expert_result.reshape(expert_count, capacity, model_width),
        "ep",
        split_axis=0,
        concat_axis=0,
        tiled=True,
    )
    picked_rows = returned.reshape(-1, model_width)[slot_index.reshape(-1)].reshape(
        tok_count, top_count, model_width
    )
    mixed_b = jnp.sum(picked_rows.astype(jnp.float32) * route_weight[:, :, None], axis=1).astype(
        jnp.bfloat16
    )
    return (mixed_a, mixed_b)


def solution(mesh):
    return jax.shard_map(
        body,
        mesh=mesh,
        in_specs=(
            P("ep", "tp"),
            P("ep", "tp"),
            P("ep", "tp"),
            P("ep", "tp"),
            P("tp"),
            P("tp", None),
            P(("ep", "tp"), None),
            P(),
            P(("ep", "tp"), None),
            P(("ep", "tp"), None),
            P("ep", None, "tp"),
            P("ep", None, "tp"),
            P("ep", "tp", None),
        ),
        out_specs=(P(("ep", "tp"), None), P(("ep", "tp"), None)),
        check_vma=False,
    )
```

profile of v0, /device:TPU:0, one launch (start us, length us, event | category | flops | bytes accessed | tf_op | source)
XLA Modules:
  0.0 468.5 jit_solution(506653708281727063)
XLA Ops:
  7.2 0.0 all-gather.2.cloned.1.call-start
  7.2 0.9 copy.48
  8.2 0.1 eq.42
  8.3 0.1 eq.38
  8.4 1.2 fusion.35
  9.7 0.6 reduce-window.38
  10.3 0.2 slice_reduce_fusion
  10.5 0.1 fusion.43
  10.6 0.1 reduce_sum.63
  10.8 0.1 copy.51
  10.8 0.1 convert_reduce_fusion
  10.9 1.7 convolution_convert_fusion.1
  12.6 44.2 %all_to_all.10 = bf16[8,48,2048]{2,1,0:T(8,128)(2,1)} all-to-all(bf16[8,48,2048]{2,1,0:T(8,128)(2,1)S(1)} %bitcast.155), channel_id=1, replica_groups=mesh['ep'=8,'tp'=4] {'ep'}, dimensions={0} | all-to-all | bytes 3145728 | tf_op jit(solution)/shard_map/all_to_all | solution.py:135
  56.8 0.0 all-gather.2.cloned.1.call-update
  56.9 0.0 reduce-scatter.5.cloned.1.call-start
  56.9 45.5 %all-gather.2.cloned.1.call-done = bf16[1536,2048]{1,0:T(8,128)(2,1)} async-done(((bf16[384,2048]{1,0:T(8,128)(2,1)}), bf16[1536,2048]{1,0:T(8,128)(2,1)}) %all-gather.2.cloned.1.call-update) | async-done | bytes 6291472 | tf_op jit(solution)/shard_map/all_gather | solution.py:136
  102.4 11.3 %fusion.19 = f32[1536,896]{1,0:T(8,128)} fusion(bf16[1536,2048]{1,0:T(8,128)(2,1)} %all-gather.2.cloned.1.call-done, bf16[1,2048,896]{2,1,0:T(8,128)(2,1)} %param.25), kind=kOutput, calls=%fused_computation.36 | convolution fusion | flops 5637144576 | bytes 15466496 | tf_op jit(solution)/shard_map/dot_general | solution.py:137
  113.7 20.1 %convolution_convert_fusion = bf16[1536,2048]{1,0:T(8,128)(2,1)} fusion(bf16[1,896,2048]{2,1,0:T(8,128)(2,1)} %param.27, f32[1536,896]{1,0:T(8,128)} %fusion.19, bf16[1536,2048]{1,0:T(8,128)(2,1)} %all-gather.2.cloned.1.call-done, bf16[1,2048,896]{2,1,0:T(8,128)(2,1)} %param.26), kind=kOutput, calls=%fused_computation.30 | convolution fusion | flops 11285692416 | bytes 25427968 | tf_op jit(solution)/shard_map/dot_general | solution.py:141
  133.9 0.0 reduce-scatter.5.cloned.1.call-update
  133.9 0.8 copy-done.9
  134.7 0.1 copy.43
  134.8 0.1 copy.42
  134.9 0.1 add.199
  135.0 0.1 copy.44
  135.2 20.5 %all_gather.14 = bf16[2048,2]{0,1:T(2,128)(2,1)S(1)} all-gather(bf16[256,2]{0,1:T(2,128)(2,1)S(1)} %copy-done.12), channel_id=1, replica_groups=mesh['ep'=8,'tp'=4] {'ep'}, dimensions={0}, use_global_device_ids=true | all-gather | bytes 9216 | tf_op jit(solution)/shard_map/all_gather | solution.py:67
  155.7 31.6 %all_gather.13 = bf16[2048,128]{0,1:T(8,128)(2,1)S(1)} all-gather(bf16[256,128]{0,1:T(8,128)(2,1)S(1)} %copy.43), channel_id=1, replica_groups=mesh['ep'=8,'tp'=4] {'ep'}, dimensions={0}, use_global_device_ids=true | all-gather | bytes 589824 | tf_op jit(solution)/shard_map/all_gather | solution.py:65
  187.3 31.7 %all_gather.12 = bf16[2048,128]{0,1:T(8,128)(2,1)S(1)} all-gather(bf16[256,128]{0,1:T(8,128)(2,1)S(1)} %copy.42), channel_id=1, replica_groups=mesh['ep'=8,'tp'=4] {'ep'}, dimensions={0}, use_global_device_ids=true | all-gather | bytes 589824 | tf_op jit(solution)/shard_map/all_gather | solution.py:66
  219.0 0.8 copy-done.6
  219.8 3.1 fusion.47
  222.8 18.6 %fusion.33 = f32[2,4,256,2,128]{2,3,4,1,0:T(2,128)S(1)} fusion(f32[2,4,256,2,128]{2,4,3,1,0:T(8,128)S(1)} %bitcast.157), kind=kOutput, calls=%fused_computation.56 | output fusion | flops 66584576 | bytes 4194304 | tf_op jit(solution)/shard_map/reduce-window.2
  241.4 1.4 copy-done.5
  242.8 0.1 reduce-window.37
  242.9 2.3 broadcast_add_fusion.1
  245.2 1.6 copy.46
  246.9 5.4 %fusion.26 = bf16[2,4,256,256]{2,3,1,0:T(8,128)(2,1)S(1)} fusion(f32[2,4,256,2,128]{2,4,3,1,0:T(8,128)} %copy.46, f32[2,256,256,4]{2,1,3,0:T(8,128)} %get-tuple-element.160, f32[2,256]{1,0:T(2,128)S(1)} %convert_bitcast_fusion.1, f32[2,4]{1,0:T(2,128)S(1)} %add.199, pred[256,256]{0,1:T(8,128)(4,1)S(1)} %iota_compare_fusion.1), kind=kLoop, calls=%fused_computation.45 | loop fusion | flops 12058624 | bytes 5310496 | tf_op jit(solution)/shard_map/convert_element_type | solution.py:36
  252.2 0.3 convolution_bitcast_fusion.1
  252.5 0.0 reduce-scatter.5.cloned.1.call-done
  252.6 4.3 all-to-all-start.1
  256.9 0.0 reduce-scatter.3.cloned.1.call-start
  256.9 5.4 %while.14 = (s32[]{:T(128)}, f32[256,2,4,64]{0,3,2,1:T(8,128)S(1)}, f32[2,4,256]{2,1,0:T(4,128)S(1)}, s32[]{:T(128)}, s32[]{:T(128)}, /*index=5*/bf16[2048,128]{...) while((s32[]{:T(128)}, f32[256,2,4,64]{0,3,2,1:T(8,128)S(1)}, ...), condition=%wide.region_7.8_spmd, body=%wide.region_3.7_spmd.sunk | while | flops 432177152 | bytes 119832520 | solution.py:105
  262.4 1.7 convolution_convert_fusion.2
  264.2 0.1 mul.91
  264.3 0.1 copy.52
  264.5 15.7 %all-to-all-done.1 = bf16[8,48,2048]{2,1,0:T(8,128)(2,1)} async-done(((bf16[8,48,2048]{2,1,0:T(8,128)(2,1)}), bf16[8,48,2048]{2,1,0:T(8,128)(2,1)}, u32[]{:S(2)}, u32[]{:S(2)}) %all-to-all-start.1) | async-done | bytes 1572896 | tf_op jit(solution)/shard_map/all_to_all | solution.py:148
  280.1 4.0 gather_fusion
  284.1 2.4 reshape.156
  286.5 5.6 %multiply_reduce_fusion = bf16[128,2048]{1,0:T(8,128)(2,1)} fusion(f32[128,2,2048]{2,1,0:T(2,128)} %reshape.156, f32[128,2]{1,0:T(8,128)S(1)} %copy.52), kind=kLoop, calls=%fused_computation.58 | loop fusion | flops 786432 | bytes 2622464 | tf_op jit(solution)/shard_map/reduce_sum | solution.py:158
  292.1 169.7 %reduce-scatter.3.cloned.1.call-done = bf16[64,2048]{1,0:T(8,128)(2,1)} async-done(((bf16[256,2048]{1,0:T(8,128)(2,1)}), bf16[64,2048]{1,0:T(8,128)(2,1)}) %reduce-scatter.3.cloned.1.call-update) | async-done | bytes 262160 | tf_op jit(solution)/shard_map/reduce_scatter | solution.py:107
  (31 shorter events, 0.2 us)
Async XLA Ops:
  7.2 255.3 %copy-start = (bf16[512,2048]{1,0:T(8,128)(2,1)S(1)}, bf16[512,2048]{1,0:T(8,128)(2,1)}, u32[]{:S(2)}) copy-start(bf16[512,2048]{1,0:T(8,128)(2,1)} %param.20) | copy-start | bytes 6291460
  7.2 95.2 %all-gather.2.cloned.1.call-start = ((), (), s32[]{:S(2)}) async-start(), calls=%async_computation.5 | async-start | bytes 7864320 | tf_op jit(solution)/shard_map/all_gather | solution.py:136
  56.9 195.7 %reduce-scatter.5.cloned.1.call-start = ((), (), s32[]{:S(2)}) async-start(), calls=%async_computation.6 | async-start | bytes 7864320 | tf_op jit(solution)/shard_map/reduce_scatter | solution.py:140
  133.8 0.8 copy-start.9
  133.8 1.0 copy-start.10
  133.8 1.1 copy-start.13
  133.8 1.2 copy-start.7
  133.9 1.3 copy-start.12
  135.1 87.7 %copy-start.8 = (bf16[256,512]{0,1:T(8,128)(2,1)}, bf16[256,512]{0,1:T(8,128)(2,1)S(1)}, u32[]{:S(2)}) copy-start(bf16[256,512]{0,1:T(8,128)(2,1)S(1)} %copy.44) | copy-start | bytes 786436
  219.0 0.8 copy-start.6
  241.4 1.4 copy-start.5
  252.6 27.6 %all-to-all-start.1 = ((bf16[8,48,2048]{2,1,0:T(8,128)(2,1)}), bf16[8,48,2048]{2,1,0:T(8,128)(2,1)}, u32[]{:S(2)}, u32[]{:S(2)}) async-start(bf16[8,48,2048]{2,1,0:T(8,128)(2,1)} %bitcast.158), calls=%async_computation.3 | async-start | bytes 3145728 | tf_op jit(solution)/shard_map/all_to_all | solution.py:148
  256.9 204.9 %reduce-scatter.3.cloned.1.call-start = ((), (), s32[]{:S(2)}) async-start(), calls=%async_computation.4 | async-start | bytes 1310720 | tf_op jit(solution)/shard_map/reduce_scatter | solution.py:107
  262.4 1.9 copy-start.11
Sparse Core Ops, SparseCore 0:
  57.0 45.3 all-gather.1
  134.0 58.8 reduce-scatter.4
  264.3 197.3 reduce-scatter.2
where the time goes:
time: 475 us; the launch traced here: 468 us
  waiting for transfers between devices  231 us (49%)
  blocking collectives  128 us (27%)
  matrix products  38.2 us (8%)
  other arithmetic  34 us (7%)
  between operations  14.2 us (3%)
  local copies, waits for them, and re-layouts  13.3 us (3%)
  loops' own time  5.43 us (1%)
    reduce_scatter x1, waiting for transfers between devices, body(): lax.psum_scatter(jnp.dot(heads_out, out_weight, preferred_element_type=jn...  170 us
    all_gather x1, waiting for transfers between devices, body(): lax.all_gather(arrived.reshape(source_rows, model_width), 'tp', axis=0, t...  45.5 us
    all_to_all x1, blocking collectives, body(): lax.all_to_all(outgoing, 'ep', split_axis=0, concat_axis=0, tiled=True)  44.2 us
    all_gather x1, blocking collectives, body(): lax.all_gather(value_rows, 'ep', axis=0, tiled=True)  31.7 us
    all_gather x1, blocking collectives, body(): lax.all_gather(key_rows, 'ep', axis=0, tiled=True)  31.6 us
    all_gather x1, blocking collectives, body(): lax.all_gather(key_bias, 'ep', axis=0, tiled=True)  20.5 us
    dot_general x1, matrix products, body(): jnp.dot(hidden_all, down_weight[0], preferred_element_type=jnp.float32)  20.1 us
    another operation x4, other arithmetic  19.2 us
  transfers between devices with their start and end apart: 4, of which 3 were waited for; matrix products, arithmetic and copies ran while one was open for 10% of the time, Pallas kernels for 0%

commit v1 on v0

v1 whole, which is shorter than its diff:
```python
import functools
import math

import jax
import jax.numpy as jnp
from jax import lax
from jax.experimental import pallas as pl
from jax.experimental.pallas import tpu as pltpu
from jax.sharding import PartitionSpec as P

HD = 64


EPSILON = 1e-06


def rms_normed(rows, gain):
    values = rows.astype(jnp.float32)
    scaled = values * lax.rsqrt(jnp.mean(values * values, axis=-1, keepdims=True) + EPSILON)
    return (scaled * gain).astype(jnp.bfloat16)


def stick_kernel(q_ref, kv_ref, tri_ref, out_ref, acc_ref, carry_ref, *, kv_local, group_size):
    block = out_ref.shape[0]
    wide = 2 * HD
    me = lax.axis_index("ep")
    acc_ref[...] = jnp.zeros_like(acc_ref)
    carry_ref[...] = jnp.zeros_like(carry_ref)
    value_width = kv_local * HD

    def tile(index, keep):
        first = pl.multiple_of(index * block, block)
        values = kv_ref[pl.ds(first, block), kv_local * wide : kv_local * wide + value_width]
        for kv in range(kv_local):
            keys = kv_ref[pl.ds(first, block), kv * wide : (kv + 1) * wide]
            for head in range(kv * group_size, (kv + 1) * group_size):
                rows = slice(head * block, (head + 1) * block)
                scores = lax.dot_general(
                    q_ref[rows, :], keys, (((1,), (1,)), ((), ())),
                    preferred_element_type=jnp.float32,
                )
                leave = jnp.maximum(scores, 0.0) + jnp.log(1.0 + jnp.exp(-jnp.abs(scores)))
                log_take = scores - leave
                if keep is not None:
                    leave = jnp.where(keep, leave, 0.0)
                high = leave.astype(jnp.bfloat16)
                low = (leave - high.astype(jnp.float32)).astype(jnp.bfloat16)
                after = jnp.dot(high, tri_ref[...], preferred_element_type=jnp.float32) + jnp.dot(
                    low, tri_ref[...], preferred_element_type=jnp.float32
                )
                carry = carry_ref[rows, :]
                weights = jnp.exp(log_take - after - carry)
                if keep is not None:
                    weights = jnp.where(keep, weights, 0.0)
                acc_ref[rows, :] += jnp.dot(
                    weights.astype(jnp.bfloat16), values, preferred_element_type=jnp.float32
                )
                carry_ref[rows, :] = carry + jnp.broadcast_to(
                    after[:, :1] + leave[:, :1], carry.shape
                )

    query_index = lax.broadcasted_iota(jnp.int32, (block, block), 0)
    key_index = lax.broadcasted_iota(jnp.int32, (block, block), 1)
    tile(me, key_index < query_index)

    def earlier(step, unused):
        tile(me - 1 - step, None)
        return unused

    lax.fori_loop(0, me, earlier, 0)
    for head in range(0, kv_local * group_size):
        kv = head // group_size
        rows = slice(head * block, (head + 1) * block)
        out_ref[:, head * HD : (head + 1) * HD] = acc_ref[rows, kv * HD : (kv + 1) * HD].astype(
            jnp.bfloat16
        )


def stick_heads(query_rows, key_rows, value_rows, key_bias, head_offset):
    block = query_rows.shape[0]
    kv_local = key_rows.shape[1] // HD
    heads = query_rows.shape[1] // HD
    group_size = heads // kv_local
    wide = 2 * HD
    one = jnp.ones((block, kv_local, 3), jnp.bfloat16)
    key_wide = jnp.concatenate(
        [
            key_rows.reshape(block, kv_local, HD),
            key_bias[:, :, None],
            one,
            jnp.zeros((block, kv_local, wide - HD - 4), jnp.bfloat16),
        ],
        axis=2,
    ).reshape(block, kv_local * wide)
    packed = jnp.concatenate([key_wide, value_rows], axis=1)
    all_packed = lax.all_gather(packed, "ep", axis=0, tiled=True)
    first = lax.reduce_precision(head_offset, 8, 7)
    second = lax.reduce_precision(head_offset - first, 8, 7)
    third = head_offset - first - second
    terms = jnp.stack([jnp.ones_like(first), first, second, third], axis=1).astype(jnp.bfloat16)
    queries = jnp.transpose(query_rows.reshape(block, heads, HD), (1, 0, 2)) * jnp.bfloat16(
        1.0 / math.sqrt(HD)
    )
    query_wide = jnp.concatenate(
        [
            queries,
            jnp.broadcast_to(terms[:, None, :], (heads, block, 4)),
            jnp.zeros((heads, block, wide - HD - 4), jnp.bfloat16),
        ],
        axis=2,
    ).reshape(heads * block, wide)
    place = jnp.arange(block)
    tri = (place[:, None] > place[None, :]).astype(jnp.bfloat16)
    span = all_packed.shape[0]
    cells = heads * block * span
    return pl.pallas_call(
        functools.partial(stick_kernel, kv_local=kv_local, group_size=group_size),
        out_shape=jax.ShapeDtypeStruct((block, heads * HD), jnp.bfloat16),
        in_specs=[pl.BlockSpec(memory_space=pltpu.VMEM)] * 3,
        out_specs=pl.BlockSpec(memory_space=pltpu.VMEM),
        scratch_shapes=[
            pltpu.VMEM((heads * block, kv_local * HD), jnp.float32),
            pltpu.VMEM((heads * block, 1), jnp.float32),
        ],
        compiler_params=pltpu.CompilerParams(vmem_limit_bytes=24 * 1024 * 1024),
        cost_estimate=pl.CostEstimate(
            flops=cells * 1000, bytes_accessed=span * 768, transcendentals=cells * 3
        ),
        name="stick",
    )(query_wide, all_packed, tri)


def body(
    query_rows,
    key_rows,
    value_rows,
    key_bias,
    head_offset,
    out_weight,
    expert_input,
    expert_gain,
    routes,
    route_weight,
    gate_weight,
    up_weight,
    down_weight,
):
    heads_out = stick_heads(query_rows, key_rows, value_rows, key_bias, head_offset)
    mixed_a = lax.psum_scatter(
        jnp.dot(heads_out, out_weight, preferred_element_type=jnp.float32).astype(jnp.bfloat16),
        "tp",
        scatter_dimension=0,
        tiled=True,
    )
    normed = rms_normed(expert_input, expert_gain)
    tok_count = normed.shape[0]
    top_count = routes.shape[1]
    model_width = normed.shape[1]
    expert_count = lax.axis_size("ep")
    capacity = max(2, 3 * tok_count * top_count // (2 * expert_count))
    flat_route = routes.reshape(-1)
    one_hot = (flat_route[:, None] == jnp.arange(expert_count)[None, :]).astype(jnp.int32)
    before = jnp.cumsum(one_hot, axis=0) - one_hot
    slot_index = (flat_route * capacity + jnp.sum(before * one_hot, axis=1)).reshape(
        tok_count, top_count
    )
    slot_ids = jnp.arange(expert_count * capacity)
    dispatch = jnp.sum(
        (slot_index[None, :, :] == slot_ids[:, None, None]).astype(jnp.int32), axis=2
    ).astype(jnp.bfloat16)
    outgoing = (
        jnp.dot(dispatch, normed, preferred_element_type=jnp.float32)
        .astype(jnp.bfloat16)
        .reshape(expert_count, capacity, model_width)
    )
    source_rows = expert_count * capacity
    arrived = lax.all_to_all(outgoing, "ep", split_axis=0, concat_axis=0, tiled=True)
    row_piece = lax.all_gather(arrived.reshape(source_rows, model_width), "tp", axis=0, tiled=True)
    gate_act = jnp.dot(row_piece, gate_weight[0], preferred_element_type=jnp.float32)
    up_act = jnp.dot(row_piece, up_weight[0], preferred_element_type=jnp.float32)
    hidden_all = (jax.nn.silu(gate_act) * up_act).astype(jnp.bfloat16)
    expert_result = lax.psum_scatter(
        jnp.dot(hidden_all, down_weight[0], preferred_element_type=jnp.float32).astype(
            jnp.bfloat16
        ),
        "tp",
        scatter_dimension=0,
        tiled=True,
    )
    returned = lax.all_to_all(
        expert_result.reshape(expert_count, capacity, model_width),
        "ep",
        split_axis=0,
        concat_axis=0,
        tiled=True,
    )
    picked_rows = returned.reshape(-1, model_width)[slot_index.reshape(-1)].reshape(
        tok_count, top_count, model_width
    )
    mixed_b = jnp.sum(picked_rows.astype(jnp.float32) * route_weight[:, :, None], axis=1).astype(
        jnp.bfloat16
    )
    return (mixed_a, mixed_b)


def solution(mesh):
    return jax.shard_map(
        body,
        mesh=mesh,
        in_specs=(
            P("ep", "tp"),
            P("ep", "tp"),
            P("ep", "tp"),
            P("ep", "tp"),
            P("tp"),
            P("tp", None),
            P(("ep", "tp"), None),
            P(),
            P(("ep", "tp"), None),
            P(("ep", "tp"), None),
            P("ep", None, "tp"),
            P("ep", None, "tp"),
            P("ep", "tp", None),
        ),
        out_specs=(P(("ep", "tp"), None), P(("ep", "tp"), None)),
        check_vma=False,
    )
```

time: 475 us -> 266 us (0.56); the launches traced: 468 us -> 265 us
  waiting for transfers between devices: 231 us -> 141 us
  blocking collectives: 128 us -> 44.2 us
  other arithmetic: 34 us -> 8.7 us
  loops' own time: 5.43 us -> 0 us
    reduce_scatter x1, waiting for transfers between devices: 170 us -> 9.92 us  [body(): lax.psum_scatter(jnp.dot(heads_out, out_weight, preferred_element_type=jn...]
    all_gather x3 -> x0, blocking collectives: 83.8 us -> none  [the longest x1 31.7 us: body(): lax.all_gather(value_rows, 'ep', axis=0, tiled=True)]
    reduce_scatter x1, waiting for transfers between devices: 0.02 us -> 56.6 us  [body(): lax.psum_scatter(jnp.dot(hidden_all, down_weight[0], preferred_element_ty...]
    another operation x5 -> x4, other arithmetic: 21.6 us -> 0.71 us
    all_to_all x1, waiting for transfers between devices: 15.7 us -> 28.8 us  [body(): lax.all_to_all(expert_result.reshape(expert_count, capacity, model_width)...]
    another operation x1 -> x0, loops' own time: 5.43 us -> none  [body(): running = lax.fori_loop(0, block_count, remote_block, running)]
    convert_element_type x2 -> x1, other arithmetic: 5.41 us -> 0.02 us  [stick_heads(): tri = (place[:, None] > place[None, :]).astype(jnp.bfloat16)]
  transfers between devices with their start and end apart: 4 -> 5, of which waited for: 3 -> 4; matrix products, arithmetic and copies ran while one was open for 10% -> 6% of each run, Pallas kernels for 0% -> 2%
where the time goes in v1:
time: 266 us; the launch traced here: 265 us
  waiting for transfers between devices  141 us (53%)
  blocking collectives  44.2 us (17%)
  matrix products  34.9 us (13%)
  between operations  15.4 us (6%)
  local copies, waits for them, and re-layouts  11.3 us (4%)
  other arithmetic  8.7 us (3%)
  starting transfers between devices  5.68 us (2%)
  Pallas kernels  4.02 us (2%)
    reduce_scatter x1, waiting for transfers between devices, body(): lax.psum_scatter(jnp.dot(hidden_all, down_weight[0], preferred_element_ty...  56.6 us
    all_gather x1, waiting for transfers between devices, body(): lax.all_gather(arrived.reshape(source_rows, model_width), 'tp', axis=0, t...  45.5 us
    all_to_all x1, blocking collectives, body(): lax.all_to_all(outgoing, 'ep', split_axis=0, concat_axis=0, tiled=True)  44.2 us
    all_to_all x1, waiting for transfers between devices, body(): lax.all_to_all(expert_result.reshape(expert_count, capacity, model_width)...  28.8 us
    dot_general x1, matrix products, body(): jnp.dot(hidden_all, down_weight[0], preferred_element_type=jnp.float32)  20.1 us
    dot_general x1, matrix products, body(): jnp.dot(row_piece, gate_weight[0], preferred_element_type=jnp.float32)  11.3 us
    reduce_scatter x1, waiting for transfers between devices, body(): lax.psum_scatter(jnp.dot(heads_out, out_weight, preferred_element_type=jn...  9.92 us
    reduce_sum x1, other arithmetic, body(): jnp.sum(picked_rows.astype(jnp.float32) * route_weight[:, :, None], axis=1)  5.59 us
  transfers between devices with their start and end apart: 5, of which 4 were waited for; matrix products, arithmetic and copies ran while one was open for 6% of the time, Pallas kernels for 2%

profile of v1, /device:TPU:0, one launch (start us, length us, event | category | flops | bytes accessed | tf_op | source)
XLA Modules:
  0.0 265.2 jit_solution(14243367296301034074)
XLA Ops:
  8.0 0.0 all-gather.5.cloned.1.call-start
  8.1 0.9 copy.45
  9.0 0.1 eq.42
  9.1 0.1 eq.38
  9.3 0.6 reduce-window.6
  9.9 0.2 slice_reduce_fusion
  10.1 0.1 fusion.16
  10.2 0.1 reduce_sum.41
  10.4 0.1 copy.48
  10.4 0.1 convert_reduce_fusion
  10.5 1.2 fusion.7
  11.8 1.7 convolution_convert_fusion.1
  13.5 44.2 %all_to_all.10 = bf16[8,48,2048]{2,1,0:T(8,128)(2,1)} all-to-all(bf16[8,48,2048]{2,1,0:T(8,128)(2,1)S(1)} %bitcast.45), channel_id=1, replica_groups=mesh['ep'=8,'tp'=4] {'ep'}, dimensions={0} | all-to-all | bytes 3145728 | tf_op jit(solution)/shard_map/all_to_all | solution.py:177
  57.7 0.0 all-gather.5.cloned.1.call-update
  57.7 0.0 reduce-scatter.5.cloned.1.call-start
  57.8 45.5 %all-gather.5.cloned.1.call-done = bf16[1536,2048]{1,0:T(8,128)(2,1)} async-done(((bf16[384,2048]{1,0:T(8,128)(2,1)}), bf16[1536,2048]{1,0:T(8,128)(2,1)}) %all-gather.5.cloned.1.call-update) | async-done | bytes 6291472 | tf_op jit(solution)/shard_map/all_gather | solution.py:178
  103.2 11.3 %fusion.4 = f32[1536,896]{1,0:T(8,128)} fusion(bf16[1536,2048]{1,0:T(8,128)(2,1)} %all-gather.5.cloned.1.call-done, bf16[1,2048,896]{2,1,0:T(8,128)(2,1)} %param.23), kind=kOutput, calls=%fused_computation.5 | convolution fusion | flops 5637144576 | bytes 15466496 | tf_op jit(solution)/shard_map/dot_general | solution.py:179
  114.5 20.1 %convolution_convert_fusion = bf16[1536,2048]{1,0:T(8,128)(2,1)} fusion(bf16[1,896,2048]{2,1,0:T(8,128)(2,1)} %param.25, f32[1536,896]{1,0:T(8,128)} %fusion.4, bf16[1536,2048]{1,0:T(8,128)(2,1)} %all-gather.5.cloned.1.call-done, bf16[1,2048,896]{2,1,0:T(8,128)(2,1)} %param.24), kind=kOutput, calls=%fused_computation.1 | convolution fusion | flops 11285692416 | bytes 25427968 | tf_op jit(solution)/shard_map/dot_general | solution.py:183
  134.7 0.0 reduce-scatter.5.cloned.1.call-update
  134.7 0.0 all-gather.3.cloned.1.call-start
  134.8 0.7 copy-done.3
  135.5 0.1 copy.42
  135.7 0.1 pad.8.clone
  135.7 0.1 pad.4.clone
  135.8 0.1 maximum_maximum_fusion.1
  135.9 0.1 copy.50
  136.0 0.7 pad_maximum_fusion
  136.7 0.0 all-gather.3.cloned.1.call-update
  136.8 0.1 pad_maximum_fusion.1
  136.9 0.1 copy.40
  137.0 0.1 copy.39
  137.2 56.6 %reduce-scatter.5.cloned.1.call-done = bf16[384,2048]{1,0:T(8,128)(2,1)} async-done(((bf16[1536,2048]{1,0:T(8,128)(2,1)}), bf16[384,2048]{1,0:T(8,128)(2,1)}) %reduce-scatter.5.cloned.1.call-update) | async-done | bytes 1572880 | tf_op jit(solution)/shard_map/reduce_scatter | solution.py:182
  193.7 5.5 %all-to-all-start.1 = ((bf16[8,48,2048]{2,1,0:T(8,128)(2,1)}), bf16[8,48,2048]{2,1,0:T(8,128)(2,1)}, u32[]{:S(2)}, u32[]{:S(2)}) async-start(bf16[8,48,2048]{2,1,0:T(8,128)(2,1)} %bitcast.46), calls=%async_computation.3 | async-start | bytes 3145728 | tf_op jit(solution)/shard_map/all_to_all | solution.py:190
  199.2 0.0 reduce-scatter.3.cloned.1.call-start
  199.3 0.1 broadcast_in_dim.10
  199.4 0.1 maximum_maximum_fusion
  199.5 0.3 copy.41
  199.8 0.0 all-gather.3.cloned.1.call-done.kv_ref
  199.9 1.4 copy-done.1
  201.3 4.0 %stick.1 = bf16[256,512]{1,0:T(8,128)(2,1)S(1)} custom-call(bf16[2048,128]{1,0:T(8,128)(2,1)S(1)} %bitcast.43, bf16[2048,384]{1,0:T(8,128)(2,1)S(1)} %copy-done.1, bf16[256,256]{1,0:T(8,128)(2,1)S(1)} %fusion.13.tri_ref), custom_call_target="tpu_custom_call" | custom-call | flops 4194304000 | bytes 1572864 | tf_op jit(solution)/shard_map/stick/pallas_call | solution.py:116
  205.3 1.7 convolution_convert_fusion.2
  207.1 0.1 mul.81
  207.2 0.1 copy.49
  207.3 28.8 %all-to-all-done.1 = bf16[8,48,2048]{2,1,0:T(8,128)(2,1)} async-done(((bf16[8,48,2048]{2,1,0:T(8,128)(2,1)}), bf16[8,48,2048]{2,1,0:T(8,128)(2,1)}, u32[]{:S(2)}, u32[]{:S(2)}) %all-to-all-start.1) | async-done | bytes 1572896 | tf_op jit(solution)/shard_map/all_to_all | solution.py:190
  236.2 4.0 %gather_fusion = bf16[256,2048]{1,0:T(8,128)(2,1)S(1)} fusion(bf16[384,2048]{1,0:T(8,128)(2,1)} %bitcast.17, s32[1024]{0:T(1024)S(1)} %pad_clamp_fusion), kind=kCustom, calls=%fused_computation | custom fusion | bytes 2098176 | tf_op jit(solution)/shard_map/gather | solution.py:197
  240.2 2.4 reshape.133
  242.5 5.6 %multiply_reduce_fusion = bf16[128,2048]{1,0:T(8,128)(2,1)} fusion(f32[128,2,2048]{2,1,0:T(2,128)} %reshape.133, f32[128,2]{1,0:T(8,128)S(1)} %copy.49), kind=kLoop, calls=%fused_computation.10 | loop fusion | flops 786432 | bytes 2622464 | tf_op jit(solution)/shard_map/reduce_sum | solution.py:200
  248.1 9.9 %reduce-scatter.3.cloned.1.call-done = bf16[64,2048]{1,0:T(8,128)(2,1)} async-done(((bf16[256,2048]{1,0:T(8,128)(2,1)}), bf16[64,2048]{1,0:T(8,128)(2,1)}) %reduce-scatter.3.cloned.1.call-update) | async-done | bytes 262160 | tf_op jit(solution)/shard_map/reduce_scatter | solution.py:149
  (29 shorter events, 0.2 us)
Async XLA Ops:
  8.0 197.3 %copy-start = (bf16[512,2048]{1,0:T(8,128)(2,1)S(1)}, bf16[512,2048]{1,0:T(8,128)(2,1)}, u32[]{:S(2)}) copy-start(bf16[512,2048]{1,0:T(8,128)(2,1)} %param.18) | copy-start | bytes 6291460
  8.0 95.2 %all-gather.5.cloned.1.call-start = ((), (), s32[]{:S(2)}) async-start(), calls=%async_computation.6 | async-start | bytes 7864320 | tf_op jit(solution)/shard_map/all_gather | solution.py:178
  57.7 136.0 %reduce-scatter.5.cloned.1.call-start = ((), (), s32[]{:S(2)}) async-start(), calls=%async_computation.7 | async-start | bytes 7864320 | tf_op jit(solution)/shard_map/reduce_scatter | solution.py:182
  134.7 0.8 copy-start.3
  134.7 1.0 copy-start.6
  134.7 1.4 copy-start.4
  134.7 2.1 copy-start.7
  134.7 2.3 copy-start.2
  134.7 65.1 %all-gather.3.cloned.1.call-start = ((), (), s32[]{:S(2)}) async-start(), calls=%async_computation.4 | async-start | bytes 1769472 | tf_op jit(solution)/shard_map/all_gather | solution.py:96
  193.7 42.5 %all-to-all-start.1 = ((bf16[8,48,2048]{2,1,0:T(8,128)(2,1)}), bf16[8,48,2048]{2,1,0:T(8,128)(2,1)}, u32[]{:S(2)}, u32[]{:S(2)}) async-start(bf16[8,48,2048]{2,1,0:T(8,128)(2,1)} %bitcast.46), calls=%async_computation.3 | async-start | bytes 3145728 | tf_op jit(solution)/shard_map/all_to_all | solution.py:190
  199.2 58.8 %reduce-scatter.3.cloned.1.call-start = ((), (), s32[]{:S(2)}) async-start(), calls=%async_computation.5 | async-start | bytes 1310720 | tf_op jit(solution)/shard_map/reduce_scatter | solution.py:149
  199.8 1.4 copy-start.1
  205.3 1.9 copy-start.5
Sparse Core Ops, SparseCore 0:
  57.8 45.3 all-gather.4
  134.9 58.8 reduce-scatter.4
  207.2 50.8 reduce-scatter.2
Sparse Core Ops, SparseCore 1:
  138.0 44.1 all-gather.2

commit v2 on v1

--- a/solution.py
+++ b/solution.py
@@ -12,6 +12,7 @@
 
 
 EPSILON = 1e-06
+CHUNKS = 2
 
 
 def rms_normed(rows, gain):
@@ -76,11 +77,9 @@
         )
 
 
-def stick_heads(query_rows, key_rows, value_rows, key_bias, head_offset):
-    block = query_rows.shape[0]
+def gather_keys(key_rows, value_rows, key_bias):
+    block = key_rows.shape[0]
     kv_local = key_rows.shape[1] // HD
-    heads = query_rows.shape[1] // HD
-    group_size = heads // kv_local
     wide = 2 * HD
     one = jnp.ones((block, kv_local, 3), jnp.bfloat16)
     key_wide = jnp.concatenate(
@@ -93,7 +92,14 @@
         axis=2,
     ).reshape(block, kv_local * wide)
     packed = jnp.concatenate([key_wide, value_rows], axis=1)
-    all_packed = lax.all_gather(packed, "ep", axis=0, tiled=True)
+    return lax.all_gather(packed, "ep", axis=0, tiled=True)
+
+
+def stick_heads(query_rows, all_packed, head_offset, kv_local):
+    block = query_rows.shape[0]
+    heads = query_rows.shape[1] // HD
+    group_size = heads // kv_local
+    wide = 2 * HD
     first = lax.reduce_precision(head_offset, 8, 7)
     second = lax.reduce_precision(head_offset - first, 8, 7)
     third = head_offset - first - second
@@ -145,62 +151,79 @@
     up_weight,
     down_weight,
 ):
-    heads_out = stick_heads(query_rows, key_rows, value_rows, key_bias, head_offset)
-    mixed_a = lax.psum_scatter(
-        jnp.dot(heads_out, out_weight, preferred_element_type=jnp.float32).astype(jnp.bfloat16),
-        "tp",
-        scatter_dimension=0,
-        tiled=True,
-    )
+    kv_local = key_rows.shape[1] // HD
+    all_packed = gather_keys(key_rows, value_rows, key_bias)
     normed = rms_normed(expert_input, expert_gain)
     tok_count = normed.shape[0]
     top_count = routes.shape[1]
     model_width = normed.shape[1]
     expert_count = lax.axis_size("ep")
     capacity = max(2, 3 * tok_count * top_count // (2 * expert_count))
+    chunks = CHUNKS if capacity % CHUNKS == 0 else 1
+    piece = capacity // chunks
     flat_route = routes.reshape(-1)
     one_hot = (flat_route[:, None] == jnp.arange(expert_count)[None, :]).astype(jnp.int32)
     before = jnp.cumsum(one_hot, axis=0) - one_hot
     slot_index = (flat_route * capacity + jnp.sum(before * one_hot, axis=1)).reshape(
         tok_count, top_count
     )
-    slot_ids = jnp.arange(expert_count * capacity)
-    dispatch = jnp.sum(
-        (slot_index[None, :, :] == slot_ids[:, None, None]).astype(jnp.int32), axis=2
-    ).astype(jnp.bfloat16)
-    outgoing = (
-        jnp.dot(dispatch, normed, preferred_element_type=jnp.float32)
-        .astype(jnp.bfloat16)
-        .reshape(expert_count, capacity, model_width)
-    )
-    source_rows = expert_count * capacity
-    arrived = lax.all_to_all(outgoing, "ep", split_axis=0, concat_axis=0, tiled=True)
-    row_piece = lax.all_gather(arrived.reshape(source_rows, model_width), "tp", axis=0, tiled=True)
-    gate_act = jnp.dot(row_piece, gate_weight[0], preferred_element_type=jnp.float32)
-    up_act = jnp.dot(row_piece, up_weight[0], preferred_element_type=jnp.float32)
-    hidden_all = (jax.nn.silu(gate_act) * up_act).astype(jnp.bfloat16)
-    expert_result = lax.psum_scatter(
-        jnp.dot(hidden_all, down_weight[0], preferred_element_type=jnp.float32).astype(
-            jnp.bfloat16
-        ),
+    chunk_rows = expert_count * piece
+    hits, arrived = [], []
+    for chunk in range(chunks):
+        slot_ids = (
+            jnp.arange(expert_count)[:, None] * capacity + chunk * piece + jnp.arange(piece)[None, :]
+        ).reshape(-1)
+        hit = slot_index[None, :, :] == slot_ids[:, None, None]
+        hits.append(hit)
+        outgoing = jnp.dot(
+            jnp.any(hit, axis=2).astype(jnp.bfloat16), normed, preferred_element_type=jnp.float32
+        ).astype(jnp.bfloat16)
+        outgoing = outgoing.reshape(expert_count, piece, model_width)
+        if chunk > 0:
+            outgoing, arrived[-1] = lax.optimization_barrier((outgoing, arrived[-1]))
+        arrived.append(lax.all_to_all(outgoing, "ep", split_axis=0, concat_axis=0, tiled=True))
+    arrived[0], all_packed = lax.optimization_barrier((arrived[0], all_packed))
+    results = []
+    for chunk in range(chunks):
+        row_piece = lax.all_gather(
+            arrived[chunk].reshape(chunk_rows, model_width), "tp", axis=0, tiled=True
+        )
+        gate_act = jnp.dot(row_piece, gate_weight[0], preferred_element_type=jnp.float32)
+        up_act = jnp.dot(row_piece, up_weight[0], preferred_element_type=jnp.float32)
+        hidden_all = (jax.nn.silu(gate_act) * up_act).astype(jnp.bfloat16)
+        partial_sum = jnp.dot(
+            hidden_all, down_weight[0], preferred_element_type=jnp.float32
+        ).astype(jnp.bfloat16)
+        if chunk == chunks - 1:
+            partial_sum, query_rows = lax.optimization_barrier((partial_sum, query_rows))
+        results.append(
+            lax.psum_scatter(partial_sum, "tp", scatter_dimension=0, tiled=True)
+        )
+    heads_out = stick_heads(query_rows, all_packed, head_offset, kv_local)
+    results[0], heads_out = lax.optimization_barrier((results[0], heads_out))
+    mixed_a = lax.psum_scatter(
+        jnp.dot(heads_out, out_weight, preferred_element_type=jnp.float32).astype(jnp.bfloat16),
         "tp",
         scatter_dimension=0,
         tiled=True,
     )
-    returned = lax.all_to_all(
-        expert_result.reshape(expert_count, capacity, model_width),
-        "ep",
-        split_axis=0,
-        concat_axis=0,
-        tiled=True,
-    )
-    picked_rows = returned.reshape(-1, model_width)[slot_index.reshape(-1)].reshape(
-        tok_count, top_count, model_width
-    )
-    mixed_b = jnp.sum(picked_rows.astype(jnp.float32) * route_weight[:, :, None], axis=1).astype(
-        jnp.bfloat16
-    )
-    return (mixed_a, mixed_b)
+    total = jnp.zeros((tok_count, model_width), jnp.float32)
+    for chunk in range(chunks):
+        returned = lax.all_to_all(
+            results[chunk].reshape(expert_count, piece, model_width),
+            "ep",
+            split_axis=0,
+            concat_axis=0,
+            tiled=True,
+        ).reshape(chunk_rows, model_width)
+        share = jnp.sum(jnp.where(hits[chunk], route_weight[None, :, :], 0.0), axis=2).T
+        for _ in range(3):
+            part = lax.reduce_precision(share, 8, 7)
+            share = share - part
+            total = total + jnp.dot(
+                part.astype(jnp.bfloat16), returned, preferred_element_type=jnp.float32
+            )
+    return (mixed_a, total.astype(jnp.bfloat16))
 
 
 def solution(mesh):

time: 266 us -> 245 us (0.921)
  waiting for transfers between devices: 141 us -> 103 us
  starting transfers between devices: 5.68 us -> 31.8 us
  matrix products: 34.9 us -> 56.9 us
  blocking collectives: 44.2 us -> 23.6 us
  local copies, waits for them, and re-layouts: 11.3 us -> 6.41 us
  other arithmetic: 8.7 us -> 4.95 us
    all_to_all x1 -> x3, starting transfers between devices: 5.52 us -> 31.4 us  [the longest x2 24.1 us: body(): lax.all_to_all(results[chunk].reshape(expert_count, piece, model_width),...]
    reduce_scatter x1 -> x2, waiting for transfers between devices: 56.6 us -> 34.1 us  [body(): lax.psum_scatter(partial_sum, 'tp', scatter_dimension=0, tiled=True)]
    all_to_all x1, blocking collectives: 44.2 us -> 23.6 us  [body(): lax.all_to_all(outgoing, 'ep', split_axis=0, concat_axis=0, tiled=True)]
    all_gather x2 -> x3, waiting for transfers between devices: 45.5 us -> 25.4 us  [the longest x2 13.8 us: body(): lax.all_gather(arrived[chunk].reshape(chunk_rows, model_width), 'tp', axi...]
    dot_general x2 -> x10, matrix products: 13 us -> 29.1 us  [the longest x2 15.8 us: body(): jnp.dot(row_piece, up_weight[0], preferred_element_type=jnp.float32)]
    all_to_all x1 -> x3, waiting for transfers between devices: 28.8 us -> 39.6 us  [the longest x1 25.7 us: body(): lax.all_to_all(outgoing, 'ep', split_axis=0, concat_axis=0, tiled=True)]
    reduce_scatter x1, waiting for transfers between devices: 9.92 us -> 3.48 us  [body(): lax.psum_scatter(jnp.dot(heads_out, out_weight, preferred_element_type=jn...]
    dot_general x1 -> x2, matrix products: 20.1 us -> 26.1 us  [body(): jnp.dot(hidden_all, down_weight[0], preferred_element_type=jnp.float32)]
  transfers between devices with their start and end apart: 5 -> 9, of which waited for: 4 -> 8; matrix products, arithmetic and copies ran while one was open for 6% -> 26% of each run, Pallas kernels for 2% -> 2%
where the time goes in v2:
time: 245 us
  waiting for transfers between devices  103 us (42%)
  matrix products  56.9 us (23%)
  starting transfers between devices  31.8 us (13%)
  blocking collectives  23.6 us (10%)
  between operations  14.4 us (6%)
  local copies, waits for them, and re-layouts  6.41 us (3%)
  other arithmetic  4.95 us (2%)
  Pallas kernels  3.82 us (2%)
    reduce_scatter x2, waiting for transfers between devices, body(): lax.psum_scatter(partial_sum, 'tp', scatter_dimension=0, tiled=True)  34.1 us
    dot_general x2, matrix products, body(): jnp.dot(hidden_all, down_weight[0], preferred_element_type=jnp.float32)  26.1 us
    all_to_all x1, waiting for transfers between devices, body(): lax.all_to_all(outgoing, 'ep', split_axis=0, concat_axis=0, tiled=True)  25.7 us
    all_to_all x2, starting transfers between devices, body(): lax.all_to_all(results[chunk].reshape(expert_count, piece, model_width),...  24.1 us
    all_to_all x1, blocking collectives, body(): lax.all_to_all(outgoing, 'ep', split_axis=0, concat_axis=0, tiled=True)  23.6 us
    dot_general x2, matrix products, body(): jnp.dot(row_piece, up_weight[0], preferred_element_type=jnp.float32)  15.8 us
    all_to_all x2, waiting for transfers between devices, body(): lax.all_to_all(results[chunk].reshape(expert_count, piece, model_width),...  13.9 us
    all_gather x2, waiting for transfers between devices, body(): lax.all_gather(arrived[chunk].reshape(chunk_rows, model_width), 'tp', axi...  13.8 us
  transfers between devices with their start and end apart: 9, of which 8 were waited for; matrix products, arithmetic and copies ran while one was open for 26% of the time, Pallas kernels for 2%

profile of v2, /device:TPU:0, one launch (start us, length us, event | category | flops | bytes accessed | tf_op | source)
XLA Modules:
  0.0 244.5 jit_solution(11018783285823752790)
XLA Ops:
  7.2 0.8 copy.56
  8.1 0.9 copy.55
  9.2 0.1 maximum_maximum_fusion.1
  9.3 0.1 copy.61
  9.4 1.5 pad_maximum_fusion
  11.0 0.8 copy.52
  11.8 0.1 eq.53
  11.9 0.1 eq.49
  12.1 0.6 reduce-window.6
  12.7 0.2 slice_reduce_fusion
  13.1 0.1 reduce_sum.39
  13.5 0.7 multiply_add_fusion
  14.2 0.1 compare_reduce_fusion
  14.4 1.2 fusion.23
  15.6 2.4 convolution_convert_fusion.1
  18.0 7.3 %all-to-all-start = ((bf16[8,24,2048]{2,1,0:T(8,128)(2,1)}), bf16[8,24,2048]{2,1,0:T(8,128)(2,1)S(1)}, u32[]{:S(2)}, u32[]{:S(2)}) async-start(bf16[8,24,2048]{2,1,0:T(8,128)(2,1)} %bitcast.95), calls=%async_computation | async-start | bytes 1572864 | tf_op jit(solution)/shard_map/all_to_all | solution.py:184
  25.4 1.3 convolution_convert_fusion.2
  26.7 25.7 %all-to-all-done = bf16[8,24,2048]{2,1,0:T(8,128)(2,1)S(1)} async-done(((bf16[8,24,2048]{2,1,0:T(8,128)(2,1)}), bf16[8,24,2048]{2,1,0:T(8,128)(2,1)S(1)}, u32[]{:S(2)}, u32[]{:S(2)}) %all-to-all-start) | async-done | bytes 786464 | tf_op jit(solution)/shard_map/all_to_all | solution.py:184
  52.5 11.6 %all-gather.4.cloned.1.call-done.kv_ref = bf16[2048,384]{1,0:T(8,128)(2,1)} async-done(((bf16[256,384]{1,0:T(8,128)(2,1)}), bf16[2048,384]{1,0:T(8,128)(2,1)}) %all-gather.4.cloned.1.call-update) | async-done | bytes 1572880 | tf_op jit(solution)/shard_map/all_gather | solution.py:95
  64.2 23.6 %all_to_all.20 = bf16[8,24,2048]{2,1,0:T(8,128)(2,1)} all-to-all(bf16[8,24,2048]{2,1,0:T(8,128)(2,1)} %bitcast.94), channel_id=1, replica_groups=mesh['ep'=8,'tp'=4] {'ep'}, dimensions={0} | all-to-all | bytes 1572864 | tf_op jit(solution)/shard_map/all_to_all | solution.py:184
  87.9 4.7 %all-gather.6.cloned.1.call-done = bf16[768,2048]{1,0:T(8,128)(2,1)} async-done(((bf16[192,2048]{1,0:T(8,128)(2,1)}), bf16[768,2048]{1,0:T(8,128)(2,1)}) %all-gather.6.cloned.1.call-update) | async-done | bytes 3145744 | tf_op jit(solution)/shard_map/all_gather | solution.py:188
  92.6 7.9 %fusion.6 = f32[768,896]{1,0:T(8,128)} fusion(bf16[768,2048]{1,0:T(8,128)(2,1)} %all-gather.6.cloned.1.call-done, bf16[1,2048,896]{2,1,0:T(8,128)(2,1)} %param.24), kind=kOutput, calls=%fused_computation.6 | convolution fusion | flops 2818572288 | bytes 9568256 | tf_op jit(solution)/shard_map/dot_general | solution.py:192
  100.5 12.9 %fusion.12 = bf16[768,2048]{1,0:T(8,128)(2,1)} fusion(bf16[1,896,2048]{2,1,0:T(8,128)(2,1)} %param.25, f32[768,896]{1,0:T(8,128)} %fusion.6, bf16[768,2048]{1,0:T(8,128)(2,1)} %all-gather.6.cloned.1.call-done, bf16[1,2048,896]{2,1,0:T(8,128)(2,1)} %param.23), kind=kOutput, calls=%fused_computation.12 | convolution fusion | flops 5642846208 | bytes 16384000 | tf_op jit(solution)/shard_map/dot_general | solution.py:194
  113.4 0.2 reduce-scatter.8.cloned.1.call-start
  113.6 9.1 %all-gather.8.cloned.1.call-done = bf16[768,2048]{1,0:T(8,128)(2,1)} async-done(((bf16[192,2048]{1,0:T(8,128)(2,1)}), bf16[768,2048]{1,0:T(8,128)(2,1)}) %all-gather.8.cloned.1.call-update) | async-done | bytes 3145744 | tf_op jit(solution)/shard_map/all_gather | solution.py:188
  122.7 7.9 %fusion.4 = f32[768,896]{1,0:T(8,128)} fusion(bf16[768,2048]{1,0:T(8,128)(2,1)} %all-gather.8.cloned.1.call-done, bf16[1,2048,896]{2,1,0:T(8,128)(2,1)} %param.24), kind=kOutput, calls=%fused_computation.4 | convolution fusion | flops 2818572288 | bytes 9568256 | tf_op jit(solution)/shard_map/dot_general | solution.py:192
  130.6 13.2 %fusion.15 = bf16[768,2048]{1,0:T(8,128)(2,1)} fusion(bf16[1,896,2048]{2,1,0:T(8,128)(2,1)} %param.25, f32[768,896]{1,0:T(8,128)} %fusion.4, bf16[768,2048]{1,0:T(8,128)(2,1)} %all-gather.8.cloned.1.call-done, bf16[1,2048,896]{2,1,0:T(8,128)(2,1)} %param.23), kind=kOutput, calls=%fused_computation.13 | convolution fusion | flops 5642846208 | bytes 16384000 | tf_op jit(solution)/shard_map/dot_general | solution.py:194
  143.8 0.6 copy-done.7
  144.6 0.1 copy-done.4
  144.7 0.1 copy.58
  145.0 0.1 maximum_maximum_fusion
  145.1 0.3 copy.60
  145.4 1.4 copy-done.1
  146.8 3.8 %stick.1 = bf16[256,512]{1,0:T(8,128)(2,1)S(1)} custom-call(bf16[2048,128]{1,0:T(8,128)(2,1)S(1)} %bitcast.91, bf16[2048,384]{1,0:T(8,128)(2,1)S(1)} %copy-done.1, bf16[256,256]{1,0:T(8,128)(2,1)S(1)} %fusion.30.tri_ref), custom_call_target="tpu_custom_call" | custom-call | flops 4194304000 | bytes 1572864 | tf_op jit(solution)/shard_map/stick/pallas_call | solution.py:122
  150.6 12.3 %reduce-scatter.4.cloned.1.call-done = bf16[192,2048]{1,0:T(8,128)(2,1)} async-done(((bf16[768,2048]{1,0:T(8,128)(2,1)}), bf16[192,2048]{1,0:T(8,128)(2,1)}) %reduce-scatter.4.cloned.1.call-update) | async-done | bytes 786448 | tf_op jit(solution)/shard_map/reduce_scatter | solution.py:200
  163.0 18.6 %all-to-all-start.2 = ((bf16[8,24,2048]{2,1,0:T(8,128)(2,1)}), bf16[8,24,2048]{2,1,0:T(8,128)(2,1)}, u32[]{:S(2)}, u32[]{:S(2)}) async-start(bf16[8,24,2048]{2,1,0:T(8,128)(2,1)} %bitcast.98), calls=%async_computation.4 | async-start | bytes 1572864 | tf_op jit(solution)/shard_map/all_to_all | solution.py:212
  181.5 21.7 %reduce-scatter.8.cloned.1.call-done = bf16[192,2048]{1,0:T(8,128)(2,1)} async-done(((bf16[768,2048]{1,0:T(8,128)(2,1)}), bf16[192,2048]{1,0:T(8,128)(2,1)}) %reduce-scatter.8.cloned.1.call-update) | async-done | bytes 786448 | tf_op jit(solution)/shard_map/reduce_scatter | solution.py:200
  203.3 5.5 %all-to-all-start.3 = ((bf16[8,24,2048]{2,1,0:T(8,128)(2,1)}), bf16[8,24,2048]{2,1,0:T(8,128)(2,1)}, u32[]{:S(2)}, u32[]{:S(2)}) async-start(bf16[8,24,2048]{2,1,0:T(8,128)(2,1)} %bitcast.97), calls=%async_computation.6 | async-start | bytes 1572864 | tf_op jit(solution)/shard_map/all_to_all | solution.py:212
  208.9 1.7 convolution_convert_fusion
  210.6 0.1 fusion.31
  210.7 1.5 fusion.41
  212.2 1.5 convolution_add_fusion.4
  213.7 1.5 convolution_add_fusion.3
  215.1 13.9 %all-to-all-done.3 = bf16[8,24,2048]{2,1,0:T(8,128)(2,1)} async-done(((bf16[8,24,2048]{2,1,0:T(8,128)(2,1)}), bf16[8,24,2048]{2,1,0:T(8,128)(2,1)}, u32[]{:S(2)}, u32[]{:S(2)}) %all-to-all-start.3) | async-done | bytes 786464 | tf_op jit(solution)/shard_map/all_to_all | solution.py:212
  229.0 1.5 convolution_add_fusion.2
  230.5 1.5 convolution_add_fusion.1
  231.9 2.3 fusion.18
  234.2 3.5 %reduce-scatter.6.cloned.1.call-done = bf16[64,2048]{1,0:T(8,128)(2,1)} async-done(((bf16[256,2048]{1,0:T(8,128)(2,1)}), bf16[64,2048]{1,0:T(8,128)(2,1)}) %reduce-scatter.6.cloned.1.call-update) | async-done | bytes 262160 | tf_op jit(solution)/shard_map/reduce_scatter | solution.py:204
  (48 shorter events, 1.3 us)
Async XLA Ops:
  7.2 201.7 %copy-start = (bf16[512,2048]{1,0:T(8,128)(2,1)S(1)}, bf16[512,2048]{1,0:T(8,128)(2,1)}, u32[]{:S(2)}) copy-start(bf16[512,2048]{1,0:T(8,128)(2,1)} %param.18) | copy-start | bytes 6291460
  7.2 18.2 %copy-start.2 = (bf16[128,2048]{1,0:T(8,128)(2,1)S(1)}, bf16[128,2048]{1,0:T(8,128)(2,1)}, u32[]{:S(2)}) copy-start(bf16[128,2048]{1,0:T(8,128)(2,1)} %param.19) | copy-start | bytes 1572868
  7.2 18.2 %copy-start.5 = (f32[2048]{0:T(1024)S(1)}, f32[2048]{0:T(1024)}, u32[]{:S(2)}) copy-start(f32[2048]{0:T(1024)} %param.20) | copy-start | bytes 24580
  7.2 56.9 %all-gather.4.cloned.1.call-start = ((), (), s32[]{:S(2)}) async-start(), calls=%async_computation.7 | async-start | bytes 1769472 | tf_op jit(solution)/shard_map/all_gather | solution.py:95
  18.0 34.4 %all-to-all-start = ((bf16[8,24,2048]{2,1,0:T(8,128)(2,1)}), bf16[8,24,2048]{2,1,0:T(8,128)(2,1)S(1)}, u32[]{:S(2)}, u32[]{:S(2)}) async-start(bf16[8,24,2048]{2,1,0:T(8,128)(2,1)} %bitcast.95), calls=%async_computation | async-start | bytes 1572864 | tf_op jit(solution)/shard_map/all_to_all | solution.py:184
  25.3 67.2 %all-gather.6.cloned.1.call-start = ((), (), s32[]{:S(2)}) async-start(), calls=%async_computation.8 | async-start | bytes 3932160 | tf_op jit(solution)/shard_map/all_gather | solution.py:188
  52.5 11.6 %copy-start.3 = (bf16[8,24,2048]{2,1,0:T(8,128)(2,1)}, bf16[8,24,2048]{2,1,0:T(8,128)(2,1)S(1)}, u32[]{:S(2)}) copy-start(bf16[8,24,2048]{2,1,0:T(8,128)(2,1)S(1)} %all-to-all-done) | copy-start | bytes 2359300
  64.1 58.5 %all-gather.8.cloned.1.call-start = ((), (), s32[]{:S(2)}) async-start(), calls=%async_computation.10 | async-start | bytes 3932160 | tf_op jit(solution)/shard_map/all_gather | solution.py:188
  87.8 75.1 %reduce-scatter.4.cloned.1.call-start = ((), (), s32[]{:S(2)}) async-start(), calls=%async_computation.9 | async-start | bytes 3932160 | tf_op jit(solution)/shard_map/reduce_scatter | solution.py:200
  113.4 89.9 %reduce-scatter.8.cloned.1.call-start = ((), (), s32[]{:S(2)}) async-start(), calls=%async_computation.12 | async-start | bytes 3932160 | tf_op jit(solution)/shard_map/reduce_scatter | solution.py:200
  143.8 0.7 copy-start.7
  143.8 1.0 copy-start.4
  145.4 1.4 copy-start.1
  163.0 40.3 %all-to-all-start.2 = ((bf16[8,24,2048]{2,1,0:T(8,128)(2,1)}), bf16[8,24,2048]{2,1,0:T(8,128)(2,1)}, u32[]{:S(2)}, u32[]{:S(2)}) async-start(bf16[8,24,2048]{2,1,0:T(8,128)(2,1)} %bitcast.98), calls=%async_computation.4 | async-start | bytes 1572864 | tf_op jit(solution)/shard_map/all_to_all | solution.py:212
  181.5 29.1 %copy-start.6 = (f32[128,2]{0,1:T(2,128)S(1)}, f32[128,2]{0,1:T(2,128)}, u32[]{:S(2)}) copy-start(f32[128,2]{0,1:T(2,128)} %param.22) | copy-start | bytes 3076
  203.3 25.7 %all-to-all-start.3 = ((bf16[8,24,2048]{2,1,0:T(8,128)(2,1)}), bf16[8,24,2048]{2,1,0:T(8,128)(2,1)}, u32[]{:S(2)}, u32[]{:S(2)}) async-start(bf16[8,24,2048]{2,1,0:T(8,128)(2,1)} %bitcast.97), calls=%async_computation.6 | async-start | bytes 1572864 | tf_op jit(solution)/shard_map/all_to_all | solution.py:212
  208.8 28.9 %reduce-scatter.6.cloned.1.call-start = ((), (), s32[]{:S(2)}) async-start(), calls=%async_computation.11 | async-start | bytes 1310720 | tf_op jit(solution)/shard_map/reduce_scatter | solution.py:204
Sparse Core Ops, SparseCore 0:
  11.1 52.9 all-gather.3
  65.7 26.8 all-gather.5
  94.1 28.4 all-gather.7
  125.1 37.8 reduce-scatter.3
  165.4 37.8 reduce-scatter.7
  212.4 25.2 reduce-scatter.5
